TPU v7x, 128 devices: a whole 4x4x4 slice. The times are simulated.
128 devices in a mesh: ra: 16 (over z, x), cb: 8 (over y, core).
Axes of the slice: x: 4, y: 4, z: 4, core: 2. Of those that a mesh axis runs over, the one named last changes fastest.
Arguments:
- inputs: bfloat16 [1536, 4096], P(None, 'ra'), may hold values from -12 to 12
- gate_weight: bfloat16 [2, 4096, 11264], P(None, 'ra', 'cb'), may hold values from -0.09375 to 0.09375
- up_weight: bfloat16 [2, 4096, 11264], P(None, 'ra', 'cb'), may hold values from -0.09375 to 0.09375
- down_weight: bfloat16 [2, 11264, 4096], P(None, 'cb', 'ra'), may hold values from -0.0546875 to 0.0546875
- norm_gain: float32 [2, 4096], P(None, 'ra'), may hold values from 0.05 to 8
- norm_shift: float32 [2, 4096], P(None, 'ra'), may hold values from -1.5 to 1.5
Outputs:
- outputs: bfloat16 [1536, 4096], P(None, 'ra')
All inputs are finite; a program needn't handle non-finite values.
Results may differ from a plain program's by a relative error of at most 0.04.
Values may be sent and summed in bfloat16 or wider, within the bound.
No kernel may reach another device: no remote copies, remote signals or barrier semaphores. Data moves between devices by JAX's collectives and lax.ppermute only.
A program may use at most 64 MiB of HBM per device.

v0:
```python
import jax
import jax.numpy as jnp
from jax import lax
from jax.sharding import Mesh
from jax.sharding import PartitionSpec as P

RESIDUAL = 0.5
EPSILON = 1e-05
BF16 = jnp.bfloat16
F32 = jnp.float32


def exchange(parts, axes):
    return lax.all_to_all(parts, axes, 0, 0, tiled=True)


def share(block, axes, peers):
    return exchange(jnp.broadcast_to(block[None], (peers, *block.shape)), axes)


def swap_core(block):
    return lax.ppermute(block, "c", [(0, 1), (1, 0)])


def dot_nt(a, b):
    return lax.dot_general(a, b, (((1,), (1,)), ((), ())), preferred_element_type=F32)


def regroup_weights(gate, up, down):
    stacked = jnp.stack((gate.T, up.T, down))
    rows = stacked.shape[1] // 4
    parts = stacked.reshape(3, 4, rows, 256).transpose(1, 0, 2, 3)
    mine = exchange(parts, "x")
    mine = mine.transpose(1, 2, 0, 3).reshape(3, rows, 1024)
    other = swap_core(mine)
    both = jnp.concatenate((mine, other), axis=1)
    return (both[:2].reshape(2 * 2 * rows, 1024), both[2])


def normed(mixed, row_sum, row_squares, gain, shift):
    mean = row_sum / 4096.0
    var = row_squares / 4096.0 - mean * mean
    out = (mixed - mean[:, None]) * lax.rsqrt(var + EPSILON)[:, None]
    return (out * gain + shift).astype(BF16)


def hidden_units(stream, w_gu):
    partial = dot_nt(stream, w_gu).astype(BF16)
    cols = partial.shape[1] // 2
    summed = exchange(partial.reshape(4, -1, 2 * cols), "z").astype(F32).sum(axis=0)
    hidden = (jax.nn.silu(summed[:, :cols]) * summed[:, cols:]).astype(BF16)
    return share(hidden, "z", 4).reshape(-1, cols)


def per_device(inputs, gate_weight, up_weight, down_weight, norm_gain, norm_shift):
    c = lax.axis_index("c")
    x = lax.axis_index("x")
    y = lax.axis_index("y")
    half = inputs.shape[0] // 2
    quarter = half // 4
    mine = lax.dynamic_slice_in_dim(inputs, c * half + y * quarter, quarter, 0)
    rows = share(mine, "x", 4).transpose(1, 0, 2).reshape(quarter, 1024)
    stream = share(rows, "y", 4).reshape(half, 1024)
    affine = jnp.stack((norm_gain[0], norm_shift[0]))
    affine = lax.all_gather(affine, "x", axis=1, tiled=True)
    gu0, down0 = regroup_weights(gate_weight[0], up_weight[0], down_weight[0])
    gu1, down1 = regroup_weights(gate_weight[1], up_weight[1], down_weight[1])
    hidden = hidden_units(stream, gu0)
    partial = jnp.dot(hidden, down0, preferred_element_type=F32).astype(BF16)
    block = half // 16
    branch = exchange(partial.reshape(16, block, 1024), ("x", "y")).astype(F32).sum(axis=0)
    own = lax.dynamic_slice_in_dim(stream, (x * 4 + y) * block, block, 0)
    mixed = RESIDUAL * own.astype(F32) + branch
    stats = lax.psum(jnp.stack((mixed.sum(axis=1), (mixed * mixed).sum(axis=1))), "z")
    out = normed(mixed, stats[0], stats[1], affine[0], affine[1])
    stream = share(out, ("x", "y"), 16).reshape(half, 1024)
    hidden = hidden_units(stream, gu1)
    partial = jnp.dot(hidden, down1, preferred_element_type=F32).astype(BF16)
    parts = partial.reshape(4, quarter, 4, 256).transpose(2, 0, 1, 3).reshape(16, quarter, 256)
    branch = exchange(parts, ("x", "y")).astype(F32).sum(axis=0)
    own = lax.dynamic_slice(stream, (y * quarter, x * 256), (quarter, 256))
    mixed = RESIDUAL * own.astype(F32) + branch
    stats = lax.psum(jnp.stack((mixed.sum(axis=1), (mixed * mixed).sum(axis=1))), ("z", "x"))
    out = normed(mixed, stats[0], stats[1], norm_gain[1], norm_shift[1])
    ours = share(out, "y", 4).reshape(half, 256)
    theirs = swap_core(ours)
    result = jnp.concatenate((ours, theirs), axis=0)
    swapped = jnp.concatenate((theirs, ours), axis=0)
    return jnp.where(c == 0, result, swapped)


def solution(mesh):
    finer = Mesh(mesh.devices.reshape(4, 4, 4, 2), ("z", "x", "y", "c"))
    ra, cb = (("z", "x"), ("y", "c"))
    in_specs = (
        P(None, ra),
        P(None, ra, cb),
        P(None, ra, cb),
        P(None, cb, ra),
        P(None, ra),
        P(None, ra),
    )
    return jax.shard_map(
        per_device, mesh=finer, in_specs=in_specs, out_specs=P(None, ra), check_vma=False
    )
```

profile of v0, /device:TPU:1, one launch (start us, length us, event | category | flops | bytes accessed | tf_op | source)
XLA Modules:
  0.0 365.9 jit_solution(2115882943331297913)
XLA Ops:
  0.0 2.4 fusion.6
  2.7 2.3 fusion.7
  5.2 2.3 fusion.8
  7.9 30.5 %all_to_all.60 = bf16[4,3,352,256]{3,2,1,0:T(8,128)(2,1)S(1)} all-to-all(bf16[4,3,352,256]{3,2,1,0:T(8,128)(2,1)S(1)} %copy.30), channel_id=1, replica_groups=mesh['z'=4,'x'=4,'y'=4,'c'=2] {'x'}, dimensions={0} | all-to-all | bytes 4325376 | tf_op jit(solution)/shard_map/all_to_all | solution.py:14
  38.7 2.2 collective-permute-start
  41.0 10.2 %all_to_all.61 = bf16[4,192,256]{2,1,0:T(8,128)(2,1)S(1)} all-to-all(bf16[4,192,256]{2,1,0:T(8,128)(2,1)S(1)} %broadcast_in_dim.14), channel_id=1, replica_groups=mesh['z'=4,'x'=4,'y'=4,'c'=2] {'x'}, dimensions={0} | all-to-all | bytes 786432 | tf_op jit(solution)/shard_map/all_to_all | solution.py:14
  51.2 1.4 broadcast_in_dim.16
  52.7 4.4 %all-to-all-start.1 = ((bf16[4,192,1024]{2,1,0:T(8,128)(2,1)}), bf16[4,192,1024]{2,1,0:T(8,128)(2,1)}, u32[]{:S(2)}, u32[]{:S(2)}) async-start(bf16[4,192,1024]{2,1,0:T(8,128)(2,1)} %broadcast_in_dim.16), calls=%async_computation.1 | async-start | bytes 3145728 | tf_op jit(solution)/shard_map/all_to_all | solution.py:14
  57.2 1.8 constant_dynamic-update-slice_fusion
  59.0 2.0 copy-done.2
  61.1 1.9 slice.96
  62.9 13.6 %all-to-all-done.1 = bf16[4,192,1024]{2,1,0:T(8,128)(2,1)} async-done(((bf16[4,192,1024]{2,1,0:T(8,128)(2,1)}), bf16[4,192,1024]{2,1,0:T(8,128)(2,1)}, u32[]{:S(2)}, u32[]{:S(2)}) %all-to-all-start.1) | async-done | bytes 1572896 | tf_op jit(solution)/shard_map/all_to_all | solution.py:14
  76.5 4.9 %convolution_convert_fusion.1 = bf16[768,1408]{1,0:T(8,128)(2,1)S(1)} fusion(bf16[768,1024]{1,0:T(8,128)(2,1)} %bitcast.1, bf16[1408,1024]{1,0:T(8,128)(2,1)} %bitcast.85), kind=kOutput, calls=%fused_computation.3 | convolution fusion | flops 2215673856 | bytes 6619136 | tf_op jit(solution)/shard_map/dot_general | solution.py:26
  81.5 29.2 %all_to_all.62 = bf16[4,192,1408]{2,1,0:T(8,128)(2,1)S(1)} all-to-all(bf16[4,192,1408]{2,1,0:T(8,128)(2,1)S(1)} %bitcast.93), channel_id=1, replica_groups=mesh['z'=4,'x'=4,'y'=4,'c'=2] {'z'}, dimensions={0} | all-to-all | bytes 4325376 | tf_op jit(solution)/shard_map/all_to_all | solution.py:14
  111.2 1.2 broadcast_in_dim.17
  112.4 4.4 %all-to-all-start.4 = ((bf16[4,192,704]{2,1,0:T(8,128)(2,1)}), bf16[4,192,704]{2,1,0:T(8,128)(2,1)}, u32[]{:S(2)}, u32[]{:S(2)}) async-start(bf16[4,192,704]{2,1,0:T(8,128)(2,1)} %broadcast_in_dim.17), calls=%async_computation.4 | async-start | bytes 2359296 | tf_op jit(solution)/shard_map/all_to_all | solution.py:14
  117.6 1.5 copy.34
  119.1 10.4 %all-to-all-done.4 = bf16[4,192,704]{2,1,0:T(8,128)(2,1)} async-done(((bf16[4,192,704]{2,1,0:T(8,128)(2,1)}), bf16[4,192,704]{2,1,0:T(8,128)(2,1)}, u32[]{:S(2)}, u32[]{:S(2)}) %all-to-all-start.4) | async-done | bytes 1081376 | tf_op jit(solution)/shard_map/all_to_all | solution.py:14
  129.5 3.6 all-to-all-start.7
  133.2 4.3 %convolution_convert_fusion.3 = bf16[768,1024]{1,0:T(8,128)(2,1)} fusion(bf16[768,704]{1,0:T(8,128)(2,1)} %bitcast.13, bf16[3,704,1024]{2,1,0:T(8,128)(2,1)} %copy-done.2), kind=kOutput, calls=%fused_computation.9 | convolution fusion | flops 1108082688 | bytes 4194304 | tf_op jit(solution)/shard_map/dot_general | solution.py:69
  137.5 18.0 %all-to-all-done.7 = bf16[4,3,352,256]{3,2,1,0:T(8,128)(2,1)S(1)} async-done(((bf16[4,3,352,256]{3,2,1,0:T(8,128)(2,1)}), bf16[4,3,352,256]{3,2,1,0:T(8,128)(2,1)S(1)}, u32[]{:S(2)}, u32[]{:S(2)}) %all-to-all-start.7) | async-done | bytes 2162720 | tf_op jit(solution)/shard_map/all_to_all | solution.py:14
  155.5 4.4 %all-to-all-start.5 = ((bf16[16,48,1024]{2,1,0:T(8,128)(2,1)}), bf16[16,48,1024]{2,1,0:T(8,128)(2,1)}, u32[]{:S(2)}, u32[]{:S(2)}) async-start(bf16[16,48,1024]{2,1,0:T(8,128)(2,1)} %bitcast.95), calls=%async_computation.5 | async-start | bytes 3145728 | tf_op jit(solution)/shard_map/all_to_all | solution.py:14
  160.0 18.8 %all_gather.3 = f32[2,1024]{1,0:T(2,128)S(1)} all-gather(f32[2,256]{1,0:T(2,128)S(1)} %pad_maximum_fusion), channel_id=1, replica_groups=mesh['z'=4,'x'=4,'y'=4,'c'=2] {'x'}, dimensions={1}, use_global_device_ids=true | all-gather | bytes 10240 | tf_op jit(solution)/shard_map/all_gather | solution.py:65
  178.8 1.6 copy.43
  180.4 8.3 %collective-permute-start.1 = (bf16[3,352,1024]{2,1,0:T(8,128)(2,1)}, bf16[3,352,1024]{2,1,0:T(8,128)(2,1)S(1)}, u32[]{:S(2)}, u32[]{:S(2)}) collective-permute-start(bf16[3,352,1024]{2,1,0:T(8,128)(2,1)} %bitcast.59), channel_id=1, source_target_pairs={{0,1},{1,0},{2,3},{3,2},{4,5},{5,4},{6,7},{7,6},{8,9},{9,8},{10,11... | collective-permute-start | bytes 6488072 | tf_op jit(solution)/shard_map/ppermute | solution.py:22
  188.8 1.7 convert_reduce_fusion.3
  190.5 1.0 fusion.2
  191.5 6.9 %psum.14 = f32[2,48]{1,0:T(2,128)S(1)} all-reduce(f32[2,48]{1,0:T(2,128)S(1)} %pad_maximum_fusion.2), channel_id=1, replica_groups=mesh['z'=4,'x'=4,'y'=4,'c'=2] {'z'}, use_global_device_ids=true, to_apply=%region_4.5 | all-reduce | flops 96 | bytes 768 | tf_op jit(solution)/shard_map/psum | solution.py:74
  199.4 1.4 broadcast_in_dim.18
  200.8 5.1 %all-to-all-start.6 = ((bf16[16,48,1024]{2,1,0:T(8,128)(2,1)}), bf16[16,48,1024]{2,1,0:T(8,128)(2,1)}, u32[]{:S(2)}, u32[]{:S(2)}) async-start(bf16[16,48,1024]{2,1,0:T(8,128)(2,1)} %broadcast_in_dim.18), calls=%async_computation.6 | async-start | bytes 3145728 | tf_op jit(solution)/shard_map/all_to_all | solution.py:14
  205.9 1.8 constant_dynamic-update-slice_fusion.3
  207.9 2.0 copy-done.3
  209.9 1.9 slice.102
  211.8 14.5 %all-to-all-done.6 = bf16[16,48,1024]{2,1,0:T(8,128)(2,1)} async-done(((bf16[16,48,1024]{2,1,0:T(8,128)(2,1)}), bf16[16,48,1024]{2,1,0:T(8,128)(2,1)}, u32[]{:S(2)}, u32[]{:S(2)}) %all-to-all-start.6) | async-done | bytes 1572896 | tf_op jit(solution)/shard_map/all_to_all | solution.py:14
  226.3 4.9 %convolution_convert_fusion = bf16[768,1408]{1,0:T(8,128)(2,1)S(1)} fusion(bf16[768,1024]{1,0:T(8,128)(2,1)} %bitcast.22, bf16[1408,1024]{1,0:T(8,128)(2,1)} %bitcast.86), kind=kOutput, calls=%fused_computation.2 | convolution fusion | flops 2215673856 | bytes 6619136 | tf_op jit(solution)/shard_map/dot_general | solution.py:26
  231.3 25.4 %all_to_all.63 = bf16[4,192,1408]{2,1,0:T(8,128)(2,1)S(1)} all-to-all(bf16[4,192,1408]{2,1,0:T(8,128)(2,1)S(1)} %bitcast.94), channel_id=1, replica_groups=mesh['z'=4,'x'=4,'y'=4,'c'=2] {'z'}, dimensions={0} | all-to-all | bytes 4325376 | tf_op jit(solution)/shard_map/all_to_all | solution.py:14
  257.4 13.7 %all_to_all.64 = bf16[4,192,704]{2,1,0:T(8,128)(2,1)S(1)} all-to-all(bf16[4,192,704]{2,1,0:T(8,128)(2,1)S(1)} %broadcast_in_dim.19), channel_id=1, replica_groups=mesh['z'=4,'x'=4,'y'=4,'c'=2] {'z'}, dimensions={0} | all-to-all | bytes 2162688 | tf_op jit(solution)/shard_map/all_to_all | solution.py:14
  271.1 3.9 %convolution_convert_fusion.2 = bf16[768,1024]{1,0:T(8,128)(2,1)} fusion(bf16[768,704]{1,0:T(8,128)(2,1)S(1)} %bitcast.100, bf16[3,704,1024]{2,1,0:T(8,128)(2,1)} %copy-done.3), kind=kOutput, calls=%fused_computation.8 | convolution fusion | flops 1108082688 | bytes 4096000 | tf_op jit(solution)/shard_map/dot_general | solution.py:78
  275.0 2.9 reshape.113
  277.9 1.4 copy.36
  279.3 10.2 %all-to-all-start.10 = ((bf16[16,192,256]{2,1,0:T(8,128)(2,1)}), bf16[16,192,256]{2,1,0:T(8,128)(2,1)S(1)}, u32[]{:S(2)}, u32[]{:S(2)}) async-start(bf16[16,192,256]{2,1,0:T(8,128)(2,1)} %bitcast.84), calls=%async_computation.10 | async-start | bytes 3145728 | tf_op jit(solution)/shard_map/all_to_all | solution.py:14
  289.6 19.0 %all-to-all-done.10 = bf16[16,192,256]{2,1,0:T(8,128)(2,1)S(1)} async-done(((bf16[16,192,256]{2,1,0:T(8,128)(2,1)}), bf16[16,192,256]{2,1,0:T(8,128)(2,1)S(1)}, u32[]{:S(2)}, u32[]{:S(2)}) %all-to-all-start.10) | async-done | bytes 1572896 | tf_op jit(solution)/shard_map/all_to_all | solution.py:14
  308.8 1.1 fusion.3
  309.9 31.9 %psum.15 = f32[2,192]{1,0:T(2,128)S(1)} all-reduce(f32[2,192]{1,0:T(2,128)S(1)} %pad_maximum_fusion.1), channel_id=1, replica_groups=mesh['z'=4,'x'=4,'y'=4,'c'=2] {'z','x'}, use_global_device_ids=true, to_apply=%region_9.10 | all-reduce | flops 384 | bytes 3072 | tf_op jit(solution)/shard_map/psum | solution.py:83
  342.9 10.1 %all_to_all.65 = bf16[4,192,256]{2,1,0:T(8,128)(2,1)S(1)} all-to-all(bf16[4,192,256]{2,1,0:T(8,128)(2,1)S(1)} %broadcast_in_dim.20), channel_id=1, replica_groups=mesh['z'=4,'x'=4,'y'=4,'c'=2] {'y'}, dimensions={0} | all-to-all | bytes 786432 | tf_op jit(solution)/shard_map/all_to_all | solution.py:14
  353.0 10.3 %collective-permute-start.2 = (bf16[768,256]{1,0:T(8,128)(2,1)S(1)}, bf16[768,256]{1,0:T(8,128)(2,1)S(1)}, u32[]{:S(2)}, u32[]{:S(2)}) collective-permute-start(bf16[768,256]{1,0:T(8,128)(2,1)S(1)} %bitcast.97), channel_id=1, source_target_pairs={{0,1},{1,0},{2,3},{3,2},{4,5},{5,4},{6,7},{7,6},{8,9},{9,8},{10,11... | collective-permute-start | bytes 1179656 | tf_op jit(solution)/shard_map/ppermute | solution.py:22
  363.3 1.3 collective-permute-done.2
  364.7 1.2 maximum_select_fusion
  (50 shorter events, 6.0 us)
Async XLA Ops:
  0.0 40.9 %copy-start = (bf16[1536,256]{1,0:T(8,128)(2,1)S(1)}, bf16[1536,256]{1,0:T(8,128)(2,1)}, u32[]{:S(2)}) copy-start(bf16[1536,256]{1,0:T(8,128)(2,1)} %param.6) | copy-start | bytes 2359300
  38.7 18.5 %collective-permute-start = (bf16[3,352,1024]{2,1,0:T(8,128)(2,1)S(1)}, bf16[3,352,1024]{2,1,0:T(8,128)(2,1)}, u32[]{:S(2)}, u32[]{:S(2)}) collective-permute-start(bf16[3,352,1024]{2,1,0:T(8,128)(2,1)S(1)} %bitcast.81), channel_id=1, source_target_pairs={{0,1},{1,0},{2,3},{3,2},{4,5},{5,4},{6,7},{7,6},{8,9},{9,8},{10,11... | collective-permute-start | bytes 6488072 | tf_op jit(solution)/shard_map/ppermute | solution.py:22
  52.7 23.9 %all-to-all-start.1 = ((bf16[4,192,1024]{2,1,0:T(8,128)(2,1)}), bf16[4,192,1024]{2,1,0:T(8,128)(2,1)}, u32[]{:S(2)}, u32[]{:S(2)}) async-start(bf16[4,192,1024]{2,1,0:T(8,128)(2,1)} %broadcast_in_dim.16), calls=%async_computation.1 | async-start | bytes 3145728 | tf_op jit(solution)/shard_map/all_to_all | solution.py:14
  59.0 2.1 copy-start.2
  111.2 5.6 %copy-start.4 = (bf16[1,256,1408]{2,1,0:T(8,128)(2,1)S(1)}, bf16[1,256,1408]{2,1,0:T(8,128)(2,1)}, u32[]{:S(2)}) copy-start(bf16[1,256,1408]{2,1,0:T(8,128)(2,1)} %get-tuple-element.9) | copy-start | bytes 2162692
  112.4 4.7 %copy-start.5 = (bf16[1,256,1408]{2,1,0:T(8,128)(2,1)S(1)}, bf16[1,256,1408]{2,1,0:T(8,128)(2,1)}, u32[]{:S(2)}) copy-start(bf16[1,256,1408]{2,1,0:T(8,128)(2,1)} %get-tuple-element.11) | copy-start | bytes 2162692
  112.4 5.0 %copy-start.6 = (bf16[1,1408,256]{2,1,0:T(8,128)(2,1)S(1)}, bf16[1,1408,256]{2,1,0:T(8,128)(2,1)}, u32[]{:S(2)}) copy-start(bf16[1,1408,256]{2,1,0:T(8,128)(2,1)} %get-tuple-element.13) | copy-start | bytes 2162692
  112.4 17.1 %all-to-all-start.4 = ((bf16[4,192,704]{2,1,0:T(8,128)(2,1)}), bf16[4,192,704]{2,1,0:T(8,128)(2,1)}, u32[]{:S(2)}, u32[]{:S(2)}) async-start(bf16[4,192,704]{2,1,0:T(8,128)(2,1)} %broadcast_in_dim.17), calls=%async_computation.4 | async-start | bytes 2359296 | tf_op jit(solution)/shard_map/all_to_all | solution.py:14
  129.5 25.9 %all-to-all-start.7 = ((bf16[4,3,352,256]{3,2,1,0:T(8,128)(2,1)}), bf16[4,3,352,256]{3,2,1,0:T(8,128)(2,1)S(1)}, u32[]{:S(2)}, u32[]{:S(2)}) async-start(bf16[4,3,352,256]{3,2,1,0:T(8,128)(2,1)} %copy.34), calls=%async_computation.7 | async-start | bytes 4325376 | tf_op jit(solution)/shard_map/all_to_all | solution.py:14
  137.5 22.4 %copy-start.7 = (f32[2,256]{1,0:T(2,128)S(1)}, f32[2,256]{1,0:T(2,128)}, u32[]{:S(2)}) copy-start(f32[2,256]{1,0:T(2,128)} %param.10) | copy-start | bytes 6148
  137.5 22.5 %copy-start.8 = (f32[2,256]{1,0:T(2,128)S(1)}, f32[2,256]{1,0:T(2,128)}, u32[]{:S(2)}) copy-start(f32[2,256]{1,0:T(2,128)} %param.11) | copy-start | bytes 6148
  155.5 33.3 %all-to-all-start.5 = ((bf16[16,48,1024]{2,1,0:T(8,128)(2,1)}), bf16[16,48,1024]{2,1,0:T(8,128)(2,1)}, u32[]{:S(2)}, u32[]{:S(2)}) async-start(bf16[16,48,1024]{2,1,0:T(8,128)(2,1)} %bitcast.95), calls=%async_computation.5 | async-start | bytes 3145728 | tf_op jit(solution)/shard_map/all_to_all | solution.py:14
  180.4 27.2 %collective-permute-start.1 = (bf16[3,352,1024]{2,1,0:T(8,128)(2,1)}, bf16[3,352,1024]{2,1,0:T(8,128)(2,1)S(1)}, u32[]{:S(2)}, u32[]{:S(2)}) collective-permute-start(bf16[3,352,1024]{2,1,0:T(8,128)(2,1)} %bitcast.59), channel_id=1, source_target_pairs={{0,1},{1,0},{2,3},{3,2},{4,5},{5,4},{6,7},{7,6},{8,9},{9,8},{10,11... | collective-permute-start | bytes 6488072 | tf_op jit(solution)/shard_map/ppermute | solution.py:22
  200.8 25.5 %all-to-all-start.6 = ((bf16[16,48,1024]{2,1,0:T(8,128)(2,1)}), bf16[16,48,1024]{2,1,0:T(8,128)(2,1)}, u32[]{:S(2)}, u32[]{:S(2)}) async-start(bf16[16,48,1024]{2,1,0:T(8,128)(2,1)} %broadcast_in_dim.18), calls=%async_computation.6 | async-start | bytes 3145728 | tf_op jit(solution)/shard_map/all_to_all | solution.py:14
  207.9 2.0 copy-start.3
  279.3 29.2 %all-to-all-start.10 = ((bf16[16,192,256]{2,1,0:T(8,128)(2,1)}), bf16[16,192,256]{2,1,0:T(8,128)(2,1)S(1)}, u32[]{:S(2)}, u32[]{:S(2)}) async-start(bf16[16,192,256]{2,1,0:T(8,128)(2,1)} %bitcast.84), calls=%async_computation.10 | async-start | bytes 3145728 | tf_op jit(solution)/shard_map/all_to_all | solution.py:14
  308.6 57.3 %copy-start.1 = (bf16[1536,256]{1,0:T(8,128)(2,1)S(1)}, bf16[1536,256]{1,0:T(8,128)(2,1)}, u32[]{:S(2)}) copy-start(bf16[1536,256]{1,0:T(8,128)(2,1)} %param.6) | copy-start | bytes 2359300
  353.0 11.7 %collective-permute-start.2 = (bf16[768,256]{1,0:T(8,128)(2,1)S(1)}, bf16[768,256]{1,0:T(8,128)(2,1)S(1)}, u32[]{:S(2)}, u32[]{:S(2)}) collective-permute-start(bf16[768,256]{1,0:T(8,128)(2,1)S(1)} %bitcast.97), channel_id=1, source_target_pairs={{0,1},{1,0},{2,3},{3,2},{4,5},{5,4},{6,7},{7,6},{8,9},{9,8},{10,11... | collective-permute-start | bytes 1179656 | tf_op jit(solution)/shard_map/ppermute | solution.py:22
where the time goes:
time: 367 us; the launch traced here: 366 us
  blocking collectives  177 us (48%)
  waiting for transfers between devices  76.9 us (21%)
  starting transfers between devices  52.9 us (14%)
  local copies, waits for them, and re-layouts  31.9 us (9%)
  matrix products  18.1 us (5%)
  other arithmetic  8.87 us (2%)
    all_to_all x6, blocking collectives, exchange(): return lax.all_to_all(parts, axes, 0, 0, tiled=True)  119 us
    all_to_all x6, waiting for transfers between devices, exchange(): return lax.all_to_all(parts, axes, 0, 0, tiled=True)  75.6 us
    all_to_all x6, starting transfers between devices, exchange(): return lax.all_to_all(parts, axes, 0, 0, tiled=True)  32.1 us
    psum x1, blocking collectives, per_device(): lax.psum(jnp.stack((mixed.sum(axis=1), (mixed * mixed).sum(axis=1))), ('z...  31.9 us
    ppermute x3, starting transfers between devices, swap_core(): return lax.ppermute(block, 'c', [(0, 1), (1, 0)])  20.8 us
    all_gather x1, blocking collectives, per_device(): affine = lax.all_gather(affine, 'x', axis=1, tiled=True)  18.8 us
    dot_general x2, matrix products, dot_nt(): lax.dot_general(a, b, (((1,), (1,)), ((), ())), preferred_element_type=F32)  9.85 us
  transfers between devices with their start and end apart: 9, of which 6 were waited for; matrix products, arithmetic and copies ran while one was open for 6% of the time, Pallas kernels for 0%

commit v1 on v0

--- a/solution.py
+++ b/solution.py
@@ -62,7 +62,8 @@
     rows = share(mine, "x", 4).transpose(1, 0, 2).reshape(quarter, 1024)
     stream = share(rows, "y", 4).reshape(half, 1024)
     affine = jnp.stack((norm_gain[0], norm_shift[0]))
-    affine = lax.all_gather(affine, "x", axis=1, tiled=True)
+    outgoing = jnp.stack([affine] * lax.axis_size("x"))
+    affine = jnp.concatenate(lax.all_to_all(outgoing, "x", 0, 0), axis=1)
     gu0, down0 = regroup_weights(gate_weight[0], up_weight[0], down_weight[0])
     gu1, down1 = regroup_weights(gate_weight[1], up_weight[1], down_weight[1])
     hidden = hidden_units(stream, gu0)

time: 367 us -> 350 us (0.954)
  blocking collectives: 177 us -> 124 us
  waiting for transfers between devices: 76.9 us -> 101 us
  starting transfers between devices: 52.9 us -> 63.1 us
    all_to_all x6 -> x5, blocking collectives: 119 us -> 85.1 us  [exchange(): return lax.all_to_all(parts, axes, 0, 0, tiled=True)]
    all_to_all x6 -> x7, waiting for transfers between devices: 75.6 us -> 95.9 us  [exchange(): return lax.all_to_all(parts, axes, 0, 0, tiled=True)]
    all_gather x1 -> x0, blocking collectives: 18.8 us -> none  [per_device(): affine = lax.all_gather(affine, 'x', axis=1, tiled=True)]
    ppermute x3, starting transfers between devices: 20.8 us -> 28.9 us  [swap_core(): return lax.ppermute(block, 'c', [(0, 1), (1, 0)])]
    all_to_all x6 -> x7, starting transfers between devices: 32.1 us -> 31 us  [exchange(): return lax.all_to_all(parts, axes, 0, 0, tiled=True)]
  transfers between devices with their start and end apart: 9 -> 11, of which waited for: 6 -> 9; matrix products, arithmetic and copies ran while one was open for 6% -> 7% of each run, Pallas kernels for 0% -> 0%
where the time goes in v1:
time: 350 us; the launch traced here: 349 us
  blocking collectives  124 us (35%)
  waiting for transfers between devices  101 us (29%)
  starting transfers between devices  63.1 us (18%)
  local copies, waits for them, and re-layouts  32.4 us (9%)
  matrix products  19.5 us (6%)
  other arithmetic  8.85 us (3%)
    all_to_all x7, waiting for transfers between devices, exchange(): return lax.all_to_all(parts, axes, 0, 0, tiled=True)  95.9 us
    all_to_all x5, blocking collectives, exchange(): return lax.all_to_all(parts, axes, 0, 0, tiled=True)  85.1 us
    psum x1, blocking collectives, per_device(): lax.psum(jnp.stack((mixed.sum(axis=1), (mixed * mixed).sum(axis=1))), ('z...  32 us
    all_to_all x7, starting transfers between devices, exchange(): return lax.all_to_all(parts, axes, 0, 0, tiled=True)  31 us
    ppermute x3, starting transfers between devices, swap_core(): return lax.ppermute(block, 'c', [(0, 1), (1, 0)])  28.9 us
    dot_general x2, matrix products, dot_nt(): lax.dot_general(a, b, (((1,), (1,)), ((), ())), preferred_element_type=F32)  11.3 us
    unnamed x24, local copies, waits for them, and re-layouts  7.07 us
    psum x1, blocking collectives, per_device(): lax.psum(jnp.stack((mixed.sum(axis=1), (mixed * mixed).sum(axis=1))), 'z')  7.02 us
  transfers between devices with their start and end apart: 11, of which 9 were waited for; matrix products, arithmetic and copies ran while one was open for 7% of the time, Pallas kernels for 0%

profile of v1, /device:TPU:1, one launch (start us, length us, event | category | flops | bytes accessed | tf_op | source)
XLA Modules:
  0.0 349.0 jit_solution(13439448667863027433)
XLA Ops:
  0.0 2.4 fusion.6
  2.6 2.3 fusion.7
  5.3 2.3 fusion.8
  7.9 30.5 %all_to_all.65 = bf16[4,3,352,256]{3,2,1,0:T(8,128)(2,1)S(1)} all-to-all(bf16[4,3,352,256]{3,2,1,0:T(8,128)(2,1)S(1)} %copy.30), channel_id=1, replica_groups=mesh['z'=4,'x'=4,'y'=4,'c'=2] {'x'}, dimensions={0} | all-to-all | bytes 4325376 | tf_op jit(solution)/shard_map/all_to_all | solution.py:14
  38.7 2.2 collective-permute-start
  41.0 10.2 %all_to_all.66 = bf16[4,192,256]{2,1,0:T(8,128)(2,1)S(1)} all-to-all(bf16[4,192,256]{2,1,0:T(8,128)(2,1)S(1)} %broadcast_in_dim.14), channel_id=1, replica_groups=mesh['z'=4,'x'=4,'y'=4,'c'=2] {'x'}, dimensions={0} | all-to-all | bytes 786432 | tf_op jit(solution)/shard_map/all_to_all | solution.py:14
  51.2 1.4 broadcast_in_dim.16
  52.7 4.3 %all-to-all-start.1 = ((bf16[4,192,1024]{2,1,0:T(8,128)(2,1)}), bf16[4,192,1024]{2,1,0:T(8,128)(2,1)}, u32[]{:S(2)}, u32[]{:S(2)}) async-start(bf16[4,192,1024]{2,1,0:T(8,128)(2,1)} %broadcast_in_dim.16), calls=%async_computation.1 | async-start | bytes 3145728 | tf_op jit(solution)/shard_map/all_to_all | solution.py:14
  57.2 1.8 constant_dynamic-update-slice_fusion
  59.0 2.0 copy-done.2
  61.0 1.9 slice.98
  62.9 13.7 %all-to-all-done.1 = bf16[4,192,1024]{2,1,0:T(8,128)(2,1)} async-done(((bf16[4,192,1024]{2,1,0:T(8,128)(2,1)}), bf16[4,192,1024]{2,1,0:T(8,128)(2,1)}, u32[]{:S(2)}, u32[]{:S(2)}) %all-to-all-start.1) | async-done | bytes 1572896 | tf_op jit(solution)/shard_map/all_to_all | solution.py:14
  76.5 6.3 %convolution_convert_fusion.1 = bf16[768,1408]{1,0:T(8,128)(2,1)} fusion(bf16[768,1024]{1,0:T(8,128)(2,1)} %bitcast.1, bf16[1408,1024]{1,0:T(8,128)(2,1)} %bitcast.86), kind=kOutput, calls=%fused_computation.3 | convolution fusion | flops 2215673856 | bytes 6619136 | tf_op jit(solution)/shard_map/dot_general | solution.py:26
  82.9 5.2 %all-to-all-start.3 = ((bf16[4,192,1408]{2,1,0:T(8,128)(2,1)}), bf16[4,192,1408]{2,1,0:T(8,128)(2,1)S(1)}, u32[]{:S(2)}, u32[]{:S(2)}) async-start(bf16[4,192,1408]{2,1,0:T(8,128)(2,1)} %bitcast.94), calls=%async_computation.3 | async-start | bytes 4325376 | tf_op jit(solution)/shard_map/all_to_all | solution.py:14
  88.1 24.6 %all-to-all-done.3 = bf16[4,192,1408]{2,1,0:T(8,128)(2,1)S(1)} async-done(((bf16[4,192,1408]{2,1,0:T(8,128)(2,1)}), bf16[4,192,1408]{2,1,0:T(8,128)(2,1)S(1)}, u32[]{:S(2)}, u32[]{:S(2)}) %all-to-all-start.3) | async-done | bytes 2162720 | tf_op jit(solution)/shard_map/all_to_all | solution.py:14
  113.3 3.2 all-to-all-start.6
  117.0 3.6 %all-to-all-done.6 = f32[4,2,256]{2,1,0:T(2,128)S(1)} async-done(((f32[4,2,256]{2,1,0:T(2,128)}), f32[4,2,256]{2,1,0:T(2,128)S(1)}, u32[]{:S(2)}, u32[]{:S(2)}) %all-to-all-start.6) | async-done | bytes 8224 | tf_op jit(solution)/shard_map/all_to_all | solution.py:66
  121.7 4.4 %all-to-all-start.4 = ((bf16[4,192,704]{2,1,0:T(8,128)(2,1)}), bf16[4,192,704]{2,1,0:T(8,128)(2,1)}, u32[]{:S(2)}, u32[]{:S(2)}) async-start(bf16[4,192,704]{2,1,0:T(8,128)(2,1)} %broadcast_in_dim.17), calls=%async_computation.4 | async-start | bytes 2359296 | tf_op jit(solution)/shard_map/all_to_all | solution.py:14
  127.0 1.5 copy.34
  128.5 9.5 %all-to-all-done.4 = bf16[4,192,704]{2,1,0:T(8,128)(2,1)} async-done(((bf16[4,192,704]{2,1,0:T(8,128)(2,1)}), bf16[4,192,704]{2,1,0:T(8,128)(2,1)}, u32[]{:S(2)}, u32[]{:S(2)}) %all-to-all-start.4) | async-done | bytes 1081376 | tf_op jit(solution)/shard_map/all_to_all | solution.py:14
  138.0 3.6 %all-to-all-start.8 = ((bf16[4,3,352,256]{3,2,1,0:T(8,128)(2,1)}), bf16[4,3,352,256]{3,2,1,0:T(8,128)(2,1)S(1)}, u32[]{:S(2)}, u32[]{:S(2)}) async-start(bf16[4,3,352,256]{3,2,1,0:T(8,128)(2,1)} %copy.34), calls=%async_computation.8 | async-start | bytes 4325376 | tf_op jit(solution)/shard_map/all_to_all | solution.py:14
  141.7 4.3 %convolution_convert_fusion.3 = bf16[768,1024]{1,0:T(8,128)(2,1)} fusion(bf16[768,704]{1,0:T(8,128)(2,1)} %bitcast.13, bf16[3,704,1024]{2,1,0:T(8,128)(2,1)} %copy-done.2), kind=kOutput, calls=%fused_computation.9 | convolution fusion | flops 1108082688 | bytes 4194304 | tf_op jit(solution)/shard_map/dot_general | solution.py:70
  145.9 16.9 %all-to-all-done.8 = bf16[4,3,352,256]{3,2,1,0:T(8,128)(2,1)S(1)} async-done(((bf16[4,3,352,256]{3,2,1,0:T(8,128)(2,1)}), bf16[4,3,352,256]{3,2,1,0:T(8,128)(2,1)S(1)}, u32[]{:S(2)}, u32[]{:S(2)}) %all-to-all-start.8) | async-done | bytes 2162720 | tf_op jit(solution)/shard_map/all_to_all | solution.py:14
  162.8 4.4 %all-to-all-start.5 = ((bf16[16,48,1024]{2,1,0:T(8,128)(2,1)}), bf16[16,48,1024]{2,1,0:T(8,128)(2,1)}, u32[]{:S(2)}, u32[]{:S(2)}) async-start(bf16[16,48,1024]{2,1,0:T(8,128)(2,1)} %bitcast.96), calls=%async_computation.5 | async-start | bytes 3145728 | tf_op jit(solution)/shard_map/all_to_all | solution.py:14
  167.2 1.7 copy.43
  168.9 6.8 %collective-permute-start.1 = (bf16[3,352,1024]{2,1,0:T(8,128)(2,1)}, bf16[3,352,1024]{2,1,0:T(8,128)(2,1)S(1)}, u32[]{:S(2)}, u32[]{:S(2)}) collective-permute-start(bf16[3,352,1024]{2,1,0:T(8,128)(2,1)} %bitcast.60), channel_id=1, source_target_pairs={{0,1},{1,0},{2,3},{3,2},{4,5},{5,4},{6,7},{7,6},{8,9},{9,8},{10,11... | collective-permute-start | bytes 6488072 | tf_op jit(solution)/shard_map/ppermute | solution.py:22
  175.7 6.9 %all-to-all-done.5 = bf16[16,48,1024]{2,1,0:T(8,128)(2,1)} async-done(((bf16[16,48,1024]{2,1,0:T(8,128)(2,1)}), bf16[16,48,1024]{2,1,0:T(8,128)(2,1)}, u32[]{:S(2)}, u32[]{:S(2)}) %all-to-all-start.5) | async-done | bytes 1572896 | tf_op jit(solution)/shard_map/all_to_all | solution.py:14
  182.6 1.7 convert_reduce_fusion.3
  185.4 7.0 %psum.14 = f32[2,48]{1,0:T(2,128)S(1)} all-reduce(f32[2,48]{1,0:T(2,128)S(1)} %pad_maximum_fusion.2), channel_id=1, replica_groups=mesh['z'=4,'x'=4,'y'=4,'c'=2] {'z'}, use_global_device_ids=true, to_apply=%region_4.5 | all-reduce | flops 96 | bytes 768 | tf_op jit(solution)/shard_map/psum | solution.py:75
  193.4 1.4 broadcast_in_dim.18
  194.8 5.3 %all-to-all-start.7 = ((bf16[16,48,1024]{2,1,0:T(8,128)(2,1)}), bf16[16,48,1024]{2,1,0:T(8,128)(2,1)}, u32[]{:S(2)}, u32[]{:S(2)}) async-start(bf16[16,48,1024]{2,1,0:T(8,128)(2,1)} %broadcast_in_dim.18), calls=%async_computation.7 | async-start | bytes 3145728 | tf_op jit(solution)/shard_map/all_to_all | solution.py:14
  200.1 1.8 constant_dynamic-update-slice_fusion.3
  202.1 2.0 copy-done.3
  204.1 1.9 slice.104
  206.0 9.4 %all-to-all-done.7 = bf16[16,48,1024]{2,1,0:T(8,128)(2,1)} async-done(((bf16[16,48,1024]{2,1,0:T(8,128)(2,1)}), bf16[16,48,1024]{2,1,0:T(8,128)(2,1)}, u32[]{:S(2)}, u32[]{:S(2)}) %all-to-all-start.7) | async-done | bytes 1572896 | tf_op jit(solution)/shard_map/all_to_all | solution.py:14
  215.4 4.9 %convolution_convert_fusion = bf16[768,1408]{1,0:T(8,128)(2,1)S(1)} fusion(bf16[768,1024]{1,0:T(8,128)(2,1)} %bitcast.23, bf16[1408,1024]{1,0:T(8,128)(2,1)} %bitcast.87), kind=kOutput, calls=%fused_computation.2 | convolution fusion | flops 2215673856 | bytes 6619136 | tf_op jit(solution)/shard_map/dot_general | solution.py:26
  220.3 19.0 %all_to_all.67 = bf16[4,192,1408]{2,1,0:T(8,128)(2,1)S(1)} all-to-all(bf16[4,192,1408]{2,1,0:T(8,128)(2,1)S(1)} %bitcast.95), channel_id=1, replica_groups=mesh['z'=4,'x'=4,'y'=4,'c'=2] {'z'}, dimensions={0} | all-to-all | bytes 4325376 | tf_op jit(solution)/shard_map/all_to_all | solution.py:14
  240.0 16.4 %all_to_all.68 = bf16[4,192,704]{2,1,0:T(8,128)(2,1)S(1)} all-to-all(bf16[4,192,704]{2,1,0:T(8,128)(2,1)S(1)} %broadcast_in_dim.19), channel_id=1, replica_groups=mesh['z'=4,'x'=4,'y'=4,'c'=2] {'z'}, dimensions={0} | all-to-all | bytes 2162688 | tf_op jit(solution)/shard_map/all_to_all | solution.py:14
  256.4 3.9 %convolution_convert_fusion.2 = bf16[768,1024]{1,0:T(8,128)(2,1)} fusion(bf16[768,704]{1,0:T(8,128)(2,1)S(1)} %bitcast.101, bf16[3,704,1024]{2,1,0:T(8,128)(2,1)} %copy-done.3), kind=kOutput, calls=%fused_computation.8 | convolution fusion | flops 1108082688 | bytes 4096000 | tf_op jit(solution)/shard_map/dot_general | solution.py:79
  260.3 2.9 reshape.124
  263.2 1.4 copy.36
  264.6 3.7 %all-to-all-start.11 = ((bf16[16,192,256]{2,1,0:T(8,128)(2,1)}), bf16[16,192,256]{2,1,0:T(8,128)(2,1)S(1)}, u32[]{:S(2)}, u32[]{:S(2)}) async-start(bf16[16,192,256]{2,1,0:T(8,128)(2,1)} %bitcast.85), calls=%async_computation.11 | async-start | bytes 3145728 | tf_op jit(solution)/shard_map/all_to_all | solution.py:14
  268.4 14.9 %all-to-all-done.11 = bf16[16,192,256]{2,1,0:T(8,128)(2,1)S(1)} async-done(((bf16[16,192,256]{2,1,0:T(8,128)(2,1)}), bf16[16,192,256]{2,1,0:T(8,128)(2,1)S(1)}, u32[]{:S(2)}, u32[]{:S(2)}) %all-to-all-start.11) | async-done | bytes 1572896 | tf_op jit(solution)/shard_map/all_to_all | solution.py:14
  284.6 32.0 %psum.15 = f32[2,192]{1,0:T(2,128)S(1)} all-reduce(f32[2,192]{1,0:T(2,128)S(1)} %pad_maximum_fusion.1), channel_id=1, replica_groups=mesh['z'=4,'x'=4,'y'=4,'c'=2] {'z','x'}, use_global_device_ids=true, to_apply=%region_9.10 | all-reduce | flops 384 | bytes 3072 | tf_op jit(solution)/shard_map/psum | solution.py:84
  317.7 8.9 %all_to_all.69 = bf16[4,192,256]{2,1,0:T(8,128)(2,1)S(1)} all-to-all(bf16[4,192,256]{2,1,0:T(8,128)(2,1)S(1)} %broadcast_in_dim.20), channel_id=1, replica_groups=mesh['z'=4,'x'=4,'y'=4,'c'=2] {'y'}, dimensions={0} | all-to-all | bytes 786432 | tf_op jit(solution)/shard_map/all_to_all | solution.py:14
  326.6 19.9 %collective-permute-start.2 = (bf16[768,256]{1,0:T(8,128)(2,1)S(1)}, bf16[768,256]{1,0:T(8,128)(2,1)S(1)}, u32[]{:S(2)}, u32[]{:S(2)}) collective-permute-start(bf16[768,256]{1,0:T(8,128)(2,1)S(1)} %bitcast.98), channel_id=1, source_target_pairs={{0,1},{1,0},{2,3},{3,2},{4,5},{5,4},{6,7},{7,6},{8,9},{9,8},{10,11... | collective-permute-start | bytes 1179656 | tf_op jit(solution)/shard_map/ppermute | solution.py:22
  346.4 1.3 collective-permute-done.2
  347.8 1.2 maximum_select_fusion
  (53 shorter events, 9.8 us)
Async XLA Ops:
  0.0 40.9 %copy-start = (bf16[1536,256]{1,0:T(8,128)(2,1)S(1)}, bf16[1536,256]{1,0:T(8,128)(2,1)}, u32[]{:S(2)}) copy-start(bf16[1536,256]{1,0:T(8,128)(2,1)} %param.6) | copy-start | bytes 2359300
  38.7 18.5 %collective-permute-start = (bf16[3,352,1024]{2,1,0:T(8,128)(2,1)S(1)}, bf16[3,352,1024]{2,1,0:T(8,128)(2,1)}, u32[]{:S(2)}, u32[]{:S(2)}) collective-permute-start(bf16[3,352,1024]{2,1,0:T(8,128)(2,1)S(1)} %bitcast.81), channel_id=1, source_target_pairs={{0,1},{1,0},{2,3},{3,2},{4,5},{5,4},{6,7},{7,6},{8,9},{9,8},{10,11... | collective-permute-start | bytes 6488072 | tf_op jit(solution)/shard_map/ppermute | solution.py:22
  52.7 23.9 %all-to-all-start.1 = ((bf16[4,192,1024]{2,1,0:T(8,128)(2,1)}), bf16[4,192,1024]{2,1,0:T(8,128)(2,1)}, u32[]{:S(2)}, u32[]{:S(2)}) async-start(bf16[4,192,1024]{2,1,0:T(8,128)(2,1)} %broadcast_in_dim.16), calls=%async_computation.1 | async-start | bytes 3145728 | tf_op jit(solution)/shard_map/all_to_all | solution.py:14
  59.0 2.0 copy-start.2
  82.9 5.2 %copy-start.7 = (f32[2,256]{1,0:T(2,128)S(1)}, f32[2,256]{1,0:T(2,128)}, u32[]{:S(2)}) copy-start(f32[2,256]{1,0:T(2,128)} %param.10) | copy-start | bytes 6148
  82.9 5.2 %copy-start.8 = (f32[2,256]{1,0:T(2,128)S(1)}, f32[2,256]{1,0:T(2,128)}, u32[]{:S(2)}) copy-start(f32[2,256]{1,0:T(2,128)} %param.11) | copy-start | bytes 6148
  82.9 29.8 %all-to-all-start.3 = ((bf16[4,192,1408]{2,1,0:T(8,128)(2,1)}), bf16[4,192,1408]{2,1,0:T(8,128)(2,1)S(1)}, u32[]{:S(2)}, u32[]{:S(2)}) async-start(bf16[4,192,1408]{2,1,0:T(8,128)(2,1)} %bitcast.94), calls=%async_computation.3 | async-start | bytes 4325376 | tf_op jit(solution)/shard_map/all_to_all | solution.py:14
  113.3 7.4 %all-to-all-start.6 = ((f32[4,2,256]{2,1,0:T(2,128)}), f32[4,2,256]{2,1,0:T(2,128)S(1)}, u32[]{:S(2)}, u32[]{:S(2)}) async-start(f32[4,2,256]{2,1,0:T(2,128)} %stack.58), calls=%async_computation.6 | async-start | bytes 16384 | tf_op jit(solution)/shard_map/all_to_all | solution.py:66
  117.0 9.1 %copy-start.4 = (bf16[1,256,1408]{2,1,0:T(8,128)(2,1)S(1)}, bf16[1,256,1408]{2,1,0:T(8,128)(2,1)}, u32[]{:S(2)}) copy-start(bf16[1,256,1408]{2,1,0:T(8,128)(2,1)} %get-tuple-element.9) | copy-start | bytes 2162692
  121.7 4.7 %copy-start.5 = (bf16[1,256,1408]{2,1,0:T(8,128)(2,1)S(1)}, bf16[1,256,1408]{2,1,0:T(8,128)(2,1)}, u32[]{:S(2)}) copy-start(bf16[1,256,1408]{2,1,0:T(8,128)(2,1)} %get-tuple-element.11) | copy-start | bytes 2162692
  121.7 5.0 %copy-start.6 = (bf16[1,1408,256]{2,1,0:T(8,128)(2,1)S(1)}, bf16[1,1408,256]{2,1,0:T(8,128)(2,1)}, u32[]{:S(2)}) copy-start(bf16[1,1408,256]{2,1,0:T(8,128)(2,1)} %get-tuple-element.13) | copy-start | bytes 2162692
  121.7 16.3 %all-to-all-start.4 = ((bf16[4,192,704]{2,1,0:T(8,128)(2,1)}), bf16[4,192,704]{2,1,0:T(8,128)(2,1)}, u32[]{:S(2)}, u32[]{:S(2)}) async-start(bf16[4,192,704]{2,1,0:T(8,128)(2,1)} %broadcast_in_dim.17), calls=%async_computation.4 | async-start | bytes 2359296 | tf_op jit(solution)/shard_map/all_to_all | solution.py:14
  138.0 24.8 %all-to-all-start.8 = ((bf16[4,3,352,256]{3,2,1,0:T(8,128)(2,1)}), bf16[4,3,352,256]{3,2,1,0:T(8,128)(2,1)S(1)}, u32[]{:S(2)}, u32[]{:S(2)}) async-start(bf16[4,3,352,256]{3,2,1,0:T(8,128)(2,1)} %copy.34), calls=%async_computation.8 | async-start | bytes 4325376 | tf_op jit(solution)/shard_map/all_to_all | solution.py:14
  162.8 19.8 %all-to-all-start.5 = ((bf16[16,48,1024]{2,1,0:T(8,128)(2,1)}), bf16[16,48,1024]{2,1,0:T(8,128)(2,1)}, u32[]{:S(2)}, u32[]{:S(2)}) async-start(bf16[16,48,1024]{2,1,0:T(8,128)(2,1)} %bitcast.96), calls=%async_computation.5 | async-start | bytes 3145728 | tf_op jit(solution)/shard_map/all_to_all | solution.py:14
  168.9 33.0 %collective-permute-start.1 = (bf16[3,352,1024]{2,1,0:T(8,128)(2,1)}, bf16[3,352,1024]{2,1,0:T(8,128)(2,1)S(1)}, u32[]{:S(2)}, u32[]{:S(2)}) collective-permute-start(bf16[3,352,1024]{2,1,0:T(8,128)(2,1)} %bitcast.60), channel_id=1, source_target_pairs={{0,1},{1,0},{2,3},{3,2},{4,5},{5,4},{6,7},{7,6},{8,9},{9,8},{10,11... | collective-permute-start | bytes 6488072 | tf_op jit(solution)/shard_map/ppermute | solution.py:22
  194.8 20.6 %all-to-all-start.7 = ((bf16[16,48,1024]{2,1,0:T(8,128)(2,1)}), bf16[16,48,1024]{2,1,0:T(8,128)(2,1)}, u32[]{:S(2)}, u32[]{:S(2)}) async-start(bf16[16,48,1024]{2,1,0:T(8,128)(2,1)} %broadcast_in_dim.18), calls=%async_computation.7 | async-start | bytes 3145728 | tf_op jit(solution)/shard_map/all_to_all | solution.py:14
  202.1 2.0 copy-start.3
  264.6 18.7 %all-to-all-start.11 = ((bf16[16,192,256]{2,1,0:T(8,128)(2,1)}), bf16[16,192,256]{2,1,0:T(8,128)(2,1)S(1)}, u32[]{:S(2)}, u32[]{:S(2)}) async-start(bf16[16,192,256]{2,1,0:T(8,128)(2,1)} %bitcast.85), calls=%async_computation.11 | async-start | bytes 3145728 | tf_op jit(solution)/shard_map/all_to_all | solution.py:14
  283.3 65.7 %copy-start.1 = (bf16[1536,256]{1,0:T(8,128)(2,1)S(1)}, bf16[1536,256]{1,0:T(8,128)(2,1)}, u32[]{:S(2)}) copy-start(bf16[1536,256]{1,0:T(8,128)(2,1)} %param.6) | copy-start | bytes 2359300
  326.6 21.2 %collective-permute-start.2 = (bf16[768,256]{1,0:T(8,128)(2,1)S(1)}, bf16[768,256]{1,0:T(8,128)(2,1)S(1)}, u32[]{:S(2)}, u32[]{:S(2)}) collective-permute-start(bf16[768,256]{1,0:T(8,128)(2,1)S(1)} %bitcast.98), channel_id=1, source_target_pairs={{0,1},{1,0},{2,3},{3,2},{4,5},{5,4},{6,7},{7,6},{8,9},{9,8},{10,11... | collective-permute-start | bytes 1179656 | tf_op jit(solution)/shard_map/ppermute | solution.py:22
